TPU v7x, 256 devices: a whole 4x4x8 slice. The times are simulated.
256 devices in a mesh: sp: 32 (over z, x), dp: 8 (over y, core).
Axes of the slice: x: 4, y: 4, z: 8, core: 2. Of those that a mesh axis runs over, the one named last changes fastest.
Arguments:
- inputs: bfloat16 [8, 8192, 2048], P('dp', 'sp'), may hold values from -6 to 6
- up_pre: bfloat16 [8, 8192, 1024], P('dp', 'sp'), may hold values from -6 to 6
- gate_pre: bfloat16 [8, 8192, 1024], P('dp', 'sp'), may hold values from -6 to 6
- cotangent: bfloat16 [8, 8192, 1024], P('dp', 'sp'), may hold values from -6 to 6
- norm_gain: float32 [1024], replicated, may hold values from 0.1 to 1.9
- up_weight: bfloat16 [2048, 1024], P('dp'), may hold values from -0.125 to 0.125
- gate_weight: bfloat16 [2048, 1024], P('dp'), may hold values from -0.125 to 0.125
- mix_weight: bfloat16 [8, 512, 512], replicated, may hold values from -0.375 to 0.375
Outputs:
- input_grad: bfloat16 [8, 8192, 2048], P('dp', 'sp')
- up_weight_grad: float32 [2048, 1024], P('dp')
- gate_weight_grad: float32 [2048, 1024], P('dp')
All inputs are finite; a program needn't handle non-finite values.
Results may differ from a plain program's by a relative error of at most 0.0064.
Values may be sent and summed in bfloat16 or wider, within the bound.
A program may use at most 128 MiB of HBM per device.

v0:
```python
import math

import jax
import jax.numpy as jnp
from jax import lax
from jax.sharding import PartitionSpec as P

GROUP_CH = 128
SPAN = 512
SEG = 64


norm_eps = 1e-05
grad_scale = 1.0 / 256.0
root_half = 1.0 / math.sqrt(2.0)
root_twopi = 1.0 / math.sqrt(2.0 * math.pi)


def side_by_side(arrays, axis, split_dim, concat_dim, along):
    both = jnp.concatenate(arrays, axis=along)
    whole, at, gathered = (
        lax.all_to_all(both, axis, split_axis=split_dim, concat_axis=concat_dim, tiled=True),
        0,
        [],
    )
    for a in arrays:
        gathered.append(lax.slice_in_dim(whole, at, at + a.shape[along], axis=along))
        at += a.shape[along]
    return tuple(gathered)


def side_by_side_2(arrays, axis, dim, along):
    widths = [a.shape[along] for a in arrays]
    both = jnp.concatenate(arrays, axis=along)
    whole = lax.all_gather(both, axis, axis=dim, tiled=True)
    return tuple(jnp.split(whole, [sum(widths[:k]) for k in range(1, len(widths))], axis=along))


def gelu_value(preact):
    return 0.5 * preact * (1.0 + lax.erf(preact * root_half))


def gelu_slope(preact):
    return (
        0.5 * (1.0 + lax.erf(preact * root_half))
        + preact * jnp.exp(-0.5 * preact * preact) * root_twopi
    )


def span_mask():
    segment = jnp.arange(SPAN) // SEG
    return segment[None, :] <= segment[:, None]


def contract(first_op, second_op):
    return lax.dot_general(
        first_op, second_op, (((1,), (1,)), ((), ())), preferred_element_type=jnp.float32
    )


def on_device(inputs, up_pre, gate_pre, cotangent, norm_gain, up_weight, gate_weight, mix_weight):
    sequences, own_rows, gated_width = cotangent.shape
    model_width = inputs.shape[2]
    up_float = up_pre.astype(jnp.float32)
    gate_float = gate_pre.astype(jnp.float32)
    grad_float = cotangent.astype(jnp.float32)
    gated_act = gelu_value(gate_float)
    centered = gated_act - jnp.mean(gated_act, axis=-1, keepdims=True)
    inverse_std = lax.rsqrt(jnp.mean(centered * centered, axis=-1, keepdims=True) + norm_eps)
    normed = centered * inverse_std
    mixer_in = (normed * norm_gain).astype(jnp.bfloat16)
    mixer_grad = (grad_float * gelu_value(up_float)).astype(jnp.bfloat16)
    arrived = side_by_side((mixer_grad, mixer_in), "sp", 2, 1, 0)
    channels = arrived[0].shape[2]
    group_index = lax.axis_index("sp") * channels // GROUP_CH
    weight_group = lax.dynamic_index_in_dim(mix_weight, group_index, 0, keepdims=False)
    masked = jnp.where(span_mask(), weight_group, jnp.zeros_like(weight_group))
    grad_blocks = arrived[0].reshape(-1, SPAN, channels)
    input_blocks = arrived[1].reshape(-1, SPAN, channels)
    spatial = jnp.einsum(
        "ts,nsc->ntc", masked, input_blocks, preferred_element_type=jnp.float32
    ).astype(jnp.bfloat16)
    normed_back = jnp.einsum(
        "ts,ntc->nsc", masked, grad_blocks, preferred_element_type=jnp.float32
    ).astype(jnp.bfloat16)
    returned = side_by_side(
        (spatial.reshape(sequences, -1, channels), normed_back.reshape(sequences, -1, channels)),
        "sp",
        1,
        2,
        0,
    )
    spatial_tokens = returned[0]
    back_tokens = returned[1]
    up_pre_grad = (grad_float * spatial_tokens.astype(jnp.float32) * gelu_slope(up_float)).astype(
        jnp.bfloat16
    )
    scaled = back_tokens.astype(jnp.float32) * norm_gain
    gated_grad = inverse_std * (
        scaled
        - jnp.mean(scaled, axis=-1, keepdims=True)
        - normed * jnp.mean(scaled * normed, axis=-1, keepdims=True)
    )
    gate_pre_grad = (gated_grad * gelu_slope(gate_float)).astype(jnp.bfloat16)
    flat_up = up_pre_grad.reshape(-1, gated_width)
    flat_gate = gate_pre_grad.reshape(-1, gated_width)
    pieces = side_by_side_2((up_weight, gate_weight), "dp", 0, 1)
    result_part = (contract(flat_up, pieces[0]) + contract(flat_gate, pieces[1])).astype(
        jnp.bfloat16
    )
    input_grad = result_part.reshape(sequences, own_rows, model_width)
    flat_inputs = inputs.reshape(-1, model_width)
    both_grads = jnp.concatenate([flat_up, flat_gate], axis=1)
    own_part = lax.psum_scatter(
        lax.dot_general(
            flat_inputs, both_grads, (((0,), (0,)), ((), ())), preferred_element_type=jnp.float32
        ),
        "dp",
        scatter_dimension=0,
        tiled=True,
    )
    weight_rows = lax.psum(own_part, "sp")
    up_weight_grad = weight_rows[:, :gated_width] * grad_scale
    gate_weight_grad = weight_rows[:, gated_width:] * grad_scale
    return (input_grad, up_weight_grad, gate_weight_grad)


def solution(mesh):
    return jax.shard_map(
        on_device,
        mesh=mesh,
        in_specs=(
            P("dp", "sp", None),
            P("dp", "sp", None),
            P("dp", "sp", None),
            P("dp", "sp", None),
            P(),
            P("dp", None),
            P("dp", None),
            P(),
        ),
        out_specs=(P("dp", "sp", None), P("dp", None), P("dp", None)),
        check_vma=False,
    )
```

profile of v0, /device:TPU:2, one launch (start us, length us, event | category | flops | bytes accessed | tf_op | source)
XLA Modules:
  0.0 473.4 jit_solution(4005701019316485023)
XLA Ops:
  7.2 0.0 copy-start
  7.2 0.0 copy-start.7
  7.2 1.3 copy.42
  8.5 1.2 copy.41
  9.8 2.0 copy.40
  11.8 0.3 fusion.39
  12.1 0.2 multiply_reduce_fusion.2
  12.4 0.0 copy-done.7
  12.4 1.6 fusion.15
  13.9 0.1 pad_maximum_fusion
  14.0 2.0 copy.43
  16.1 11.7 %all-to-all-start = ((bf16[2,256,1024]{1,0,2:T(2,128)(2,1)}), bf16[2,256,1024]{1,0,2:T(2,128)(2,1)}, u32[]{:S(2)}, u32[]{:S(2)}) async-start(bf16[2,256,1024]{1,0,2:T(2,128)(2,1)} %copy.43), calls=%async_computation | async-start | bytes 2097152 | tf_op jit(solution)/shard_map/all_to_all | solution.py:22
  27.8 28.1 %all-to-all-done = bf16[2,256,1024]{1,0,2:T(2,128)(2,1)} async-done(((bf16[2,256,1024]{1,0,2:T(2,128)(2,1)}), bf16[2,256,1024]{1,0,2:T(2,128)(2,1)}, u32[]{:S(2)}, u32[]{:S(2)}) %all-to-all-start) | async-done | bytes 1048608 | tf_op jit(solution)/shard_map/all_to_all | solution.py:22
  55.9 1.4 copy.44
  57.3 0.9 fusion.53
  58.1 1.1 copy.45
  59.2 2.0 reshape.269
  61.2 1.8 fusion.13
  63.0 1.1 copy.47
  64.1 2.1 reshape.270
  66.2 2.1 copy.48
  68.3 2.0 reshape.271
  70.3 1.8 fusion.14
  72.2 1.1 copy.50
  73.3 2.1 reshape.272
  75.3 2.3 pad_maximum_fusion.1
  77.6 9.2 %copy.51 = bf16[2,8192,32]{2,0,1:T(2,128)(2,1)} copy(bf16[2,8192,32]{1,2,0:T(8,128)(2,1)} %pad_maximum_fusion.1) | data formatting | bytes 2097152 | tf_op jit(solution)/shard_map/concatenate | solution.py:20
  86.8 9.9 %reshape.280 = bf16[32,2,8192]{2,1,0:T(2,128)(2,1)} reshape(bf16[8192,2,32]{2,1,0:T(2,128)(2,1)} %bitcast.49) | data formatting | bytes 2097152
  96.7 5.6 %all-to-all-start.1 = ((bf16[32,2,8192]{2,1,0:T(2,128)(2,1)}), bf16[32,2,8192]{2,1,0:T(2,128)(2,1)}, u32[]{:S(2)}, u32[]{:S(2)}) async-start(bf16[32,2,8192]{2,1,0:T(2,128)(2,1)} %reshape.280), calls=%async_computation.1 | async-start | bytes 2097152 | tf_op jit(solution)/shard_map/all_to_all | solution.py:22
  102.3 0.2 reduce-scatter.2.cloned.1.call-start
  102.6 0.1 mul.153
  102.6 0.1 copy.55
  102.7 26.7 %all-to-all-done.1 = bf16[32,2,8192]{2,1,0:T(2,128)(2,1)} async-done(((bf16[32,2,8192]{2,1,0:T(2,128)(2,1)}), bf16[32,2,8192]{2,1,0:T(2,128)(2,1)}, u32[]{:S(2)}, u32[]{:S(2)}) %all-to-all-start.1) | async-done | bytes 1048608 | tf_op jit(solution)/shard_map/all_to_all | solution.py:22
  129.4 10.0 %reshape.281 = bf16[8192,2,32]{2,1,0:T(2,128)(2,1)} reshape(bf16[32,2,8192]{2,1,0:T(2,128)(2,1)} %all-to-all-done.1) | data formatting | bytes 2097152
  139.4 7.1 %copy.58 = bf16[2,32,256,32]{2,1,3,0:T(8,128)(2,1)} copy(bf16[2,32,256,32]{3,0,2,1:T(2,128)(2,1)} %bitcast.50) | data formatting | bytes 2097152 | tf_op jit(solution)/shard_map/all_to_all | solution.py:22
  146.5 1.5 slice_convert_fusion.1
  148.0 1.3 multiply_reduce_fusion.1
  149.3 0.6 copy.53
  149.9 0.0 copy-done.2
  149.9 0.5 fusion.17
  150.4 0.0 copy-start.3
  150.4 0.6 copy.54
  151.1 0.3 multiply_reduce_fusion
  151.4 0.7 fusion.31
  152.1 0.0 copy-done.3
  152.1 8.1 %convolution_bitcast_fusion = f32[2048,2048]{0,1:T(8,128)} fusion(bf16[256,1024]{0,1:T(8,128)(2,1)S(1)} %bitcast.55, bf16[256,1024]{0,1:T(8,128)(2,1)S(1)} %bitcast.54, bf16[1,256,2048]{2,1,0:T(8,128)(2,1)S(1)} %copy-done), kind=kOutput, calls=%fused_computation | convolution fusion | flops 2149580800 | bytes 18874368 | tf_op jit(solution)/shard_map/dot_general | solution.py:115
  160.2 0.0 reduce-scatter.2.cloned.1.call-update
  160.2 0.0 all-gather.2.cloned.1.call-start
  160.3 1.0 copy-done.5
  161.2 0.2 copy-done.6
  161.4 1.1 pad_maximum_fusion.2
  162.4 0.0 all-gather.2.cloned.1.call-update
  162.5 0.0 all-reduce.2.cloned.1.call-start
  162.5 89.1 %reduce-scatter.2.cloned.1.call-done = f32[256,2048]{0,1:T(8,128)} async-done(((f32[2048,2048]{0,1:T(8,128)}), f32[256,2048]{0,1:T(8,128)}) %reduce-scatter.2.cloned.1.call-update) | async-done | bytes 2097168 | tf_op jit(solution)/shard_map/reduce_scatter | solution.py:114
  251.6 0.0 all-reduce.2.cloned.1.call-update
  251.6 0.0 copy-start.4
  251.6 54.3 %all-gather.2.cloned.1.call-done = bf16[2048,2048]{1,0:T(8,128)(2,1)} async-done(((bf16[256,2048]{1,0:T(8,128)(2,1)}), bf16[2048,2048]{1,0:T(8,128)(2,1)}) %all-gather.2.cloned.1.call-update) | async-done | bytes 8388624 | tf_op jit(solution)/shard_map/all_gather | solution.py:35
  305.9 3.5 fusion
  309.4 0.0 copy-start.1
  309.4 4.6 fusion.10
  314.0 148.6 %all-reduce.2.cloned.1.call-done = f32[256,2048]{0,1:T(8,128)} async-done(((f32[256,2048]{0,1:T(8,128)}), f32[256,2048]{0,1:T(8,128)}) %all-reduce.2.cloned.1.call-update) | async-done | bytes 2097168 | tf_op jit(solution)/shard_map/psum | solution.py:122
  462.6 1.7 slice_multiply_fusion
  464.3 1.3 copy.57
  465.6 1.3 copy.56
  (11 shorter events, 0.0 us)
Async XLA Ops:
  7.2 144.9 %copy-start = (bf16[1,256,2048]{2,1,0:T(8,128)(2,1)S(1)}, bf16[1,256,2048]{2,1,0:T(8,128)(2,1)}, u32[]{:S(2)}) copy-start(bf16[1,256,2048]{2,1,0:T(8,128)(2,1)} %param.8) | copy-start | bytes 3145732
  7.2 5.2 %copy-start.7 = (f32[1024]{0:T(1024)S(1)}, f32[1024]{0:T(1024)}, u32[]{:S(2)}) copy-start(f32[1024]{0:T(1024)} %param.12) | copy-start | bytes 12292
  16.1 39.8 %all-to-all-start = ((bf16[2,256,1024]{1,0,2:T(2,128)(2,1)}), bf16[2,256,1024]{1,0,2:T(2,128)(2,1)}, u32[]{:S(2)}, u32[]{:S(2)}) async-start(bf16[2,256,1024]{1,0,2:T(2,128)(2,1)} %copy.43), calls=%async_computation | async-start | bytes 2097152 | tf_op jit(solution)/shard_map/all_to_all | solution.py:22
  96.7 32.7 %all-to-all-start.1 = ((bf16[32,2,8192]{2,1,0:T(2,128)(2,1)}), bf16[32,2,8192]{2,1,0:T(2,128)(2,1)}, u32[]{:S(2)}, u32[]{:S(2)}) async-start(bf16[32,2,8192]{2,1,0:T(2,128)(2,1)} %reshape.280), calls=%async_computation.1 | async-start | bytes 2097152 | tf_op jit(solution)/shard_map/all_to_all | solution.py:22
  102.3 149.3 %reduce-scatter.2.cloned.1.call-start = ((), (), s32[]{:S(2)}) async-start(), calls=%async_computation.4 | async-start | bytes 18874368 | tf_op jit(solution)/shard_map/reduce_scatter | solution.py:114
  146.5 3.4 copy-start.2
  150.4 1.6 copy-start.3
  160.2 1.0 copy-start.5
  160.2 1.2 copy-start.6
  160.2 145.7 %all-gather.2.cloned.1.call-start = ((), (), s32[]{:S(2)}) async-start(), calls=%async_computation.3 | async-start | bytes 9437184 | tf_op jit(solution)/shard_map/all_gather | solution.py:35
  162.5 300.1 %all-reduce.2.cloned.1.call-start = ((), (), s32[]{:S(2)}) async-start(), calls=%async_computation.5 | async-start | bytes 4194304 | tf_op jit(solution)/shard_map/psum | solution.py:122
  251.6 57.8 %copy-start.4 = (bf16[1,256,1024]{1,2,0:T(8,128)(2,1)S(1)}, bf16[1,256,1024]{1,2,0:T(8,128)(2,1)}, u32[]{:S(2)}) copy-start(bf16[1,256,1024]{1,2,0:T(8,128)(2,1)} %copy-done.3) | copy-start | bytes 1572868
  309.4 157.4 %copy-start.1 = (bf16[1,256,2048]{2,1,0:T(8,128)(2,1)S(1)}, bf16[1,256,2048]{2,1,0:T(8,128)(2,1)}, u32[]{:S(2)}) copy-start(bf16[1,256,2048]{2,1,0:T(8,128)(2,1)} %param.8) | copy-start | bytes 3145732
Sparse Core Ops, SparseCore 0:
  160.3 91.2 reduce-scatter.1
  254.0 51.8 all-gather.1
  309.5 153.0 all-reduce.1
where the time goes:
time: 476 us; the launch traced here: 473 us
  waiting for transfers between devices  347 us (73%)
  local copies, waits for them, and re-layouts  63.8 us (13%)
  matrix products  19.8 us (4%)
  starting transfers between devices  17.6 us (4%)
  between operations  14 us (3%)
  other arithmetic  11.5 us (2%)
    psum x1, waiting for transfers between devices, on_device(): weight_rows = lax.psum(own_part, 'sp')  149 us
    reduce_scatter x1, waiting for transfers between devices, on_device(): lax.psum_scatter(lax.dot_general(flat_inputs, both_grads, (((0,), (0,)),...  89.1 us
    all_to_all x2, waiting for transfers between devices, side_by_side(): lax.all_to_all(both, axis, split_axis=split_dim, concat_axis=concat_dim,...  54.8 us
    all_gather x1, waiting for transfers between devices, side_by_side_2(): whole = lax.all_gather(both, axis, axis=dim, tiled=True)  54.3 us
    unnamed x23, local copies, waits for them, and re-layouts  28.3 us
    all_to_all x2, starting transfers between devices, side_by_side(): lax.all_to_all(both, axis, split_axis=split_dim, concat_axis=concat_dim,...  17.3 us
    concatenate x2, local copies, waits for them, and re-layouts, side_by_side(): both = jnp.concatenate(arrays, axis=along)  11.2 us
  transfers between devices with their start and end apart: 5, of which 5 were waited for; matrix products, arithmetic and copies ran while one was open for 2% of the time, Pallas kernels for 0%

commit v1 on v0

v1 whole, which is shorter than its diff:
```python
import math

import jax
import jax.numpy as jnp
from jax import lax
from jax.experimental import pallas as pl
from jax.experimental.pallas import tpu as pltpu
from jax.sharding import PartitionSpec as P

MESH = pl.DeviceIdType.MESH
NX, NY, NZ = 4, 4, 8
ROWS = 256
GATED = 1024
MODEL = 2048
NG = 8
CH = 128
SEG = 64
f32, bf16 = jnp.float32, jnp.bfloat16

norm_eps = 1e-05
grad_scale = 1.0 / 256.0
root_half = 1.0 / math.sqrt(2.0)
root_twopi = 1.0 / math.sqrt(2.0 * math.pi)


def dot(a, b):
    return jnp.dot(a, b, preferred_element_type=f32)


def dot_t(a, b):
    return lax.dot_general(a, b, (((1,), (1,)), ((), ())), preferred_element_type=f32)


class Names:
    def __init__(self):
        self.at = {}

    def __call__(self, *key):
        return self.at.setdefault(key, len(self.at))


N_REMOTE = 160
N_LOCAL = 16


def kernel(
    x_hbm, up_hbm, gate_hbm, cot_hbm, gain_hbm, wu_hbm, wg_hbm, mix_hbm,
    ig_out, du_out, dg_out,
    upv, gatev, cotv, gainv, xo, xp, xt, mixd, mixo, mixin, peer, acc, back, cs, nrm, si,
    gu, gg, wb, outv, uorg, urec, uredf, uredb, uy, uyf, uyb, ux, agu,
    gorg, grec, gredf, gredb, gy, gyf, gyb, gz, agg, duv, dgv,
    send_sem, recv_sem, loc_sem,
):
    sp, dp = lax.axis_index("sp"), lax.axis_index("dp")
    z, x = sp // NX, sp % NX
    y, c = dp // 2, dp % 2
    h = x % 2

    def dev(dz=0, dx=0, dy=0, other=False):
        zz, xx, yy = (z + dz + NZ) % NZ, (x + dx + NX) % NX, (y + dy + NY) % NY
        cc = 1 - c if other else c
        return {"sp": zz * NX + xx, "dp": yy * 2 + cc}

    pair_dev = {"sp": z * NX + (x + 1 - 2 * h), "dp": dp}
    names, started = Names(), []

    def remote(key, src, dst, to):
        i = names(*key)
        return pltpu.make_async_remote_copy(
            src_ref=src, dst_ref=dst, send_sem=send_sem.at[i], recv_sem=recv_sem.at[i],
            device_id=to, device_id_type=MESH,
        )

    def send(key, src, dst, to):
        copy = remote(key, src, dst, to)
        copy.start()
        started.append(copy)

    def arrive(key, dst):
        remote(key, dst, dst, pair_dev).wait_recv()

    loads = {}

    def load(name, src, dst):
        copy = pltpu.make_async_copy(src, dst, loc_sem.at[len(loads)])
        copy.start()
        loads[name] = copy

    load("gate", gate_hbm.at[0], gatev)
    load("up", up_hbm.at[0], upv)
    load("cot", cot_hbm.at[0], cotv)
    load("gain", gain_hbm, gainv)
    off = pl.multiple_of(h * ROWS, ROWS)
    load("mixd", mix_hbm.at[:, pl.ds(off, ROWS), pl.ds(off, ROWS)], mixd)
    load("mixo", mix_hbm.at[:, pl.ds(ROWS, ROWS), pl.ds(0, ROWS)], mixo)

    def columns(block):
        return pl.ds(pl.multiple_of(block * ROWS, ROWS), ROWS)

    for k in range(NY):
        load(("x", k), x_hbm.at[0, :, columns(2 * k + c)], xo.at[k])
    load("wu", wu_hbm, wb.at[dp, 0])
    load("wg", wg_hbm, wb.at[dp, 1])

    peers = [dev(other=True)]
    peers += [dev(dy=k) for k in range(1, NY)]
    peers += [dev(dx=k) for k in range(1, NX)]
    peers += [dev(dz=k) for k in range(1, NZ)]
    barrier = pltpu.get_barrier_semaphore()
    for p in peers:
        pl.semaphore_signal(barrier, inc=1, device_id=p, device_id_type=MESH)
    pl.semaphore_wait(barrier, len(peers))

    up_w, gate_w = wu_hbm, wg_hbm
    mine = {0: up_w, 1: gate_w}
    for d, order in ((1, (0, 1)), (-1, (1, 0))):
        for part in order:
            send(("w", d, part), mine[part], wb.at[dp, part], dev(dy=d))
    for k in range(NY):
        send(("xp", k), x_hbm.at[0, :, columns(2 * k + 1 - c)], xp.at[k], dev(other=True))
    for part in range(2):
        send(("wc", 0, part), mine[part], wb.at[dp, part], dev(other=True))

    def block_of(dy, other=False):
        return ((y + dy + NY) % NY) * 2 + (1 - c if other else c)

    def weights_first():
        for d, part in ((1, 0), (-1, 1)):
            b = block_of(-d)
            arrive(("w", d, part), wb.at[b, part])
            send(("wf", d), wb.at[b, part], wb.at[b, part], dev(dy=d))
            send(("wc", -d, part), wb.at[b, part], wb.at[b, part], dev(other=True))

    def weights_second():
        for d, part in ((1, 1), (-1, 0)):
            b = block_of(-d)
            arrive(("w", d, part), wb.at[b, part])
            send(("wc", -d, part), wb.at[b, part], wb.at[b, part], dev(other=True))

    def weights_third():
        b = block_of(2)
        for d, part in ((1, 0), (-1, 1)):
            arrive(("wf", d), wb.at[b, part])
            send(("wc", 2, part), wb.at[b, part], wb.at[b, part], dev(other=True))

    def weights_other(dy):
        b = block_of(dy, True)
        for part in range(2):
            arrive(("wc", dy, part), wb.at[b, part])

    RB = 16
    for name in ("gate", "up", "cot", "gain"):
        loads[name].wait()

    def gate_rows(i, _):
        rows = pl.ds(pl.multiple_of(i * RB, RB), RB)
        a = gatev[rows, :].astype(f32)
        cdf = 0.5 * (1.0 + lax.erf(a * root_half))
        act = a * cdf
        centered = act - jnp.mean(act, axis=-1, keepdims=True)
        inv = lax.rsqrt(jnp.mean(centered * centered, axis=-1, keepdims=True) + norm_eps)
        normed = centered * inv
        nrm[rows, :] = normed
        si[rows, :] = inv * (cdf + a * jnp.exp(-0.5 * a * a) * root_twopi)
        value = (normed * gainv[...]).astype(bf16)
        for g in range(NG):
            mixin[0, g, rows, :] = value[:, g * CH : (g + 1) * CH]
        return 0

    def up_rows(i, _):
        rows = pl.ds(pl.multiple_of(i * RB, RB), RB)
        a = upv[rows, :].astype(f32)
        ct = cotv[rows, :].astype(f32)
        cdf = 0.5 * (1.0 + lax.erf(a * root_half))
        value = (ct * (a * cdf)).astype(bf16)
        slope = ct * (cdf + a * jnp.exp(-0.5 * a * a) * root_twopi)
        for g in range(NG):
            mixin[1, g, rows, :] = value[:, g * CH : (g + 1) * CH]
            cs[g, rows, :] = slope[:, g * CH : (g + 1) * CH]
        return 0

    lax.fori_loop(0, ROWS // RB, gate_rows, 0)
    lax.fori_loop(0, ROWS // RB, up_rows, 0)
    for g in range(NG):
        send(("pair", g), mixin.at[h, g], peer.at[g], pair_dev)

    loads["mixd"].wait()
    loads["mixo"].wait()
    seg_t = lax.broadcasted_iota(jnp.int32, (ROWS, ROWS), 0) // SEG
    seg_s = lax.broadcasted_iota(jnp.int32, (ROWS, ROWS), 1) // SEG
    keep = seg_s <= seg_t

    def diag(g):
        return jnp.where(keep, mixd[g].astype(f32), 0.0)

    def up_grad(g, spatial):
        gu[g, 0:ROWS, :] = (spatial.astype(bf16).astype(f32) * cs[g]).astype(bf16)

    def gate_grads():
        def rows_of(i, _):
            rows = pl.ds(pl.multiple_of(i * RB, RB), RB)
            nb = jnp.concatenate([back[g, rows, :] for g in range(NG)], axis=1)
            scaled = nb.astype(f32) * gainv[...]
            normed = nrm[rows, :]
            m1 = jnp.mean(scaled, axis=-1, keepdims=True)
            m2 = jnp.mean(scaled * normed, axis=-1, keepdims=True)
            grad = ((scaled - m1 - normed * m2) * si[rows, :]).astype(bf16)
            for k in range(NX):
                gg[k, rows, :] = grad[:, k * 256 : (k + 1) * 256]
            return 0

        lax.fori_loop(0, ROWS // RB, rows_of, 0)

    @pl.when(h == 0)
    def _():
        def step(g, _):
            d = diag(g)
            up_grad(g, dot(d.astype(bf16), mixin[0, g]))
            acc[g] = dot(d.T.astype(bf16), mixin[1, g])
            return 0

        lax.fori_loop(0, NG, step, 0)

    @pl.when(h == 1)
    def _():
        def step(g, _):
            d = diag(g)
            back[g] = dot(d.T.astype(bf16), mixin[1, g]).astype(bf16)
            acc[g] = dot(d.astype(bf16), mixin[0, g])
            return 0

        lax.fori_loop(0, NG, step, 0)
        gate_grads()

    for k in range(NY):
        loads[("x", k)].wait()
        xt[k, :, 0:ROWS] = xo[k].T
        arrive(("xp", k), xp.at[k])
        xt[k, :, ROWS : 2 * ROWS] = xp[k].T

    for g in range(NG):
        arrive(("pair", g), peer.at[g])

        @pl.when(h == 0)
        def _():
            back[g] = (acc[g] + dot(mixo[g].astype(f32).T.astype(bf16), peer[g])).astype(bf16)

        @pl.when(h == 1)
        def _():
            up_grad(g, acc[g] + dot(mixo[g], peer[g]))

    @pl.when(h == 0)
    def _():
        gate_grads()

    own, theirs = pl.ds(0, ROWS), pl.ds(ROWS, ROWS)
    send(("gu",), gu.at[:, own, :], gu.at[:, theirs, :], dev(other=True))
    send(("gg",), gg.at[:, own, :], gg.at[:, theirs, :], dev(other=True))
    arrive(("gu",), gu.at[:, theirs, :])
    arrive(("gg",), gg.at[:, theirs, :])

    def u_term(k, j):
        return dot(xt[k], gu[j])

    def g_term(k, j):
        return dot(xt[k], gg[j])

    def halves(d):
        long = 0 if d == 1 else 1
        return long, 1 - long

    def zi(v):
        return (z + v + NZ) % NZ

    def xi(v):
        return (x + v + NX) % NX

    di = {1: 0, -1: 1}

    def fill(dst, slot, term, half, j, add=None):
        for r in range(2):
            t = term(2 * half + r, j)
            if add is not None:
                t = t + add[slot, r].astype(f32)
            dst[slot, r] = t.astype(bf16)

    USLOT = {("L", k): k for k in range(4)} | {("S", k): 4 + k for k in range(3)}
    GSLOT = {("L", k): k for k in range(2)} | {("S", 0): 2}

    def u_slot(d, kind, k):
        return di[d] * 7 + USLOT[kind, k]

    def g_slot(d, kind, k):
        return di[d] * 3 + GSLOT[kind, k]

    def u_start():
        for kind, dist in (("L", 4), ("S", 3)):
            for d in (1, -1):
                half = halves(d)[0 if kind == "L" else 1]
                slot = di[d] * 2 + (0 if kind == "L" else 1)
                fill(uorg, slot, u_term, half, zi(d * dist))
                send(("u", d, kind, dist - 1), uorg.at[slot], urec.at[u_slot(d, kind, dist - 1)], dev(dz=d))

    def u_step(kind, k):
        for d in (1, -1):
            half = halves(d)[0 if kind == "L" else 1]
            slot = u_slot(d, kind, k)
            arrive(("u", d, kind, k), urec.at[slot])
            fill(urec, slot, u_term, half, zi(d * k), add=urec)
            send(("u", d, kind, k - 1), urec.at[slot], urec.at[u_slot(d, kind, k - 1)], dev(dz=d))

    def g_start():
        for kind, dist in (("L", 2), ("S", 1)):
            for d in (1, -1):
                half = halves(d)[0 if kind == "L" else 1]
                slot = di[d] * 2 + (0 if kind == "L" else 1)
                fill(gorg, slot, g_term, half, xi(d * dist))
                send(("g", d, kind, dist - 1), gorg.at[slot], grec.at[g_slot(d, kind, dist - 1)], dev(dx=d))

    def g_step(kind, k):
        for d in (1, -1):
            half = halves(d)[0 if kind == "L" else 1]
            slot = g_slot(d, kind, k)
            arrive(("g", d, kind, k), grec.at[slot])
            fill(grec, slot, g_term, half, xi(d * k), add=grec)
            send(("g", d, kind, k - 1), grec.at[slot], grec.at[g_slot(d, kind, k - 1)], dev(dx=d))

    def u_end():
        for d, kind in ((1, "S"), (-1, "S"), (1, "L"), (-1, "L")):
            arrive(("u", d, kind, 0), urec.at[u_slot(d, kind, 0)])
        for half in range(2):
            plus = u_slot(1, "L" if half == 0 else "S", 0)
            minus = u_slot(-1, "L" if half == 1 else "S", 0)
            for r in range(2):
                k = 2 * half + r
                t = u_term(k, z) + urec[plus, r].astype(f32) + urec[minus, r].astype(f32)
                uredf[k] = t
                uredb[k] = t.astype(bf16)
        for k in range(1, NY):
            to = (y + k) % NY
            send(("uy", k), uredb.at[to], uy.at[k - 1], dev(dy=k))

    def g_end():
        for d, kind in ((1, "S"), (-1, "S"), (1, "L"), (-1, "L")):
            arrive(("g", d, kind, 0), grec.at[g_slot(d, kind, 0)])
        for half in range(2):
            plus = g_slot(1, "L" if half == 0 else "S", 0)
            minus = g_slot(-1, "L" if half == 1 else "S", 0)
            for r in range(2):
                k = 2 * half + r
                t = g_term(k, x) + grec[plus, r].astype(f32) + grec[minus, r].astype(f32)
                gredf[k] = t
                gredb[k] = t.astype(bf16)
        for k in range(1, NY):
            to = (y + k) % NY
            send(("gy", k), gredb.at[to], gy.at[k - 1], dev(dy=k))

    def u_y():
        for k in range(1, NY):
            arrive(("uy", k), uy.at[k - 1])
        t = uredf[y]
        for k in range(1, NY):
            t = t + uy[k - 1].astype(f32)
        for k in range(NX):
            piece = t[k * 64 : (k + 1) * 64, :]
            uyf[k] = piece
            uyb[k] = piece.astype(bf16)
        for k in range(1, NX):
            send(("ux", k), uyb.at[xi(k)], ux.at[k - 1], dev(dx=k))

    def u_x():
        for k in range(1, NX):
            arrive(("ux", k), ux.at[k - 1])
        t = uyf[x]
        for k in range(1, NX):
            t = t + ux[k - 1].astype(f32)
        agu[x, z] = (t * grad_scale).astype(bf16)
        for k in range(1, NZ):
            send(("au", k), agu.at[x, z], agu.at[x, z], dev(dz=k))

    def g_y():
        for k in range(1, NY):
            arrive(("gy", k), gy.at[k - 1])
        t = gredf[y]
        for k in range(1, NY):
            t = t + gy[k - 1].astype(f32)
        for k in range(NZ):
            piece = t[k * 32 : (k + 1) * 32, :]
            gyf[k] = piece
            gyb[k] = piece.astype(bf16)
        for k in range(1, NZ):
            send(("gz", k), gyb.at[zi(k)], gz.at[k - 1], dev(dz=k))

    def g_z():
        for k in range(1, NZ):
            arrive(("gz", k), gz.at[k - 1])
        t = gyf[z]
        for k in range(1, NZ):
            t = t + gz[k - 1].astype(f32)
        agg[x, z] = (t * grad_scale).astype(bf16)
        for k in range(1, NZ):
            send(("ag", k), agg.at[x, z], agg.at[x, z], dev(dz=k))

    def gather_z(tag, buf):
        for k in range(1, NZ):
            arrive((tag, k), buf.at[x, zi(-k)])
        for d in (1, -1):
            send((tag, "x", d), buf.at[x], buf.at[x], dev(dx=d))

    def part_of(d):
        return pl.ds(0, NZ // 2) if d == 1 else pl.ds(NZ // 2, NZ // 2)

    def gather_x(tag, buf):
        for d in (1, -1):
            arrive((tag, "x", d), buf.at[xi(-d)])
            send((tag, "xx", d), buf.at[xi(-d), part_of(d)], buf.at[xi(-d), part_of(d)], dev(dx=d))

    def gather_last(tag, buf):
        for d in (1, -1):
            arrive((tag, "xx", d), buf.at[xi(2), part_of(d)])

    def out_block(b):
        lu = jnp.concatenate([gu[g, 0:ROWS, :] for g in range(NG)], axis=1)
        lg = jnp.concatenate([gg[g, 0:ROWS, :] for g in range(NX)], axis=1)
        t = dot_t(lu, wb[b, 0]) + dot_t(lg, wb[b, 1])
        outv[b] = t.astype(bf16)

    stores = []

    def store_block(b, i):
        copy = pltpu.make_async_copy(outv.at[b], ig_out.at[:, columns(b)], loc_sem.at[i])
        copy.start()
        stores.append(copy)

    u_start()
    g_start()
    weights_first()
    u_step("L", 3)
    g_step("L", 1)
    u_step("S", 2)
    u_step("L", 2)
    loads["wu"].wait()
    loads["wg"].wait()
    weights_second()
    u_step("S", 1)
    u_step("L", 1)
    g_end()
    u_end()
    out_block(block_of(0))
    weights_third()
    u_y()
    g_y()
    weights_other(0)
    out_block(block_of(0, True))
    out_block(block_of(1))
    u_x()
    g_z()
    out_block(block_of(3))
    gather_z("au", agu)
    gather_z("ag", agg)
    out_block(block_of(2))
    weights_other(1)
    out_block(block_of(1, True))
    gather_x("au", agu)
    gather_x("ag", agg)
    weights_other(-1)
    out_block(block_of(3, True))
    weights_other(2)
    out_block(block_of(2, True))
    for b in range(8):
        store_block(b, b)
    gather_last("au", agu)
    for i in range(NX):
        for j in range(NZ):
            duv[i * 64 : (i + 1) * 64, j * CH : (j + 1) * CH] = agu[i, j].astype(f32)
    copy = pltpu.make_async_copy(duv, du_out, loc_sem.at[8])
    copy.start()
    stores.append(copy)
    gather_last("ag", agg)
    for i in range(NX):
        for j in range(NZ):
            dgv[j * 32 : (j + 1) * 32, i * 256 : (i + 1) * 256] = agg[i, j].astype(f32)
    copy = pltpu.make_async_copy(dgv, dg_out, loc_sem.at[9])
    copy.start()
    stores.append(copy)
    for copy in started:
        copy.wait_send()
    for copy in stores:
        copy.wait()
    assert len(names.at) <= N_REMOTE and len(loads) <= N_LOCAL


def on_device(inputs, up_pre, gate_pre, cotangent, norm_gain, up_weight, gate_weight, mix_weight):
    V = pltpu.VMEM
    scratch = [
        V((ROWS, GATED), bf16), V((ROWS, GATED), bf16), V((ROWS, GATED), bf16), V((1, GATED), f32),
        V((NY, ROWS, ROWS), bf16), V((NY, ROWS, ROWS), bf16), V((NY, ROWS, 2 * ROWS), bf16),
        V((NG, ROWS, ROWS), bf16), V((NG, ROWS, ROWS), bf16),
        V((2, NG, ROWS, CH), bf16), V((NG, ROWS, CH), bf16), V((NG, ROWS, CH), f32), V((NG, ROWS, CH), bf16),
        V((NG, ROWS, CH), f32), V((ROWS, GATED), f32), V((ROWS, GATED), f32),
        V((NG, 2 * ROWS, CH), bf16), V((NX, 2 * ROWS, 256), bf16),
        V((8, 2, ROWS, GATED), bf16), V((8, ROWS, ROWS), bf16),
        V((4, 2, ROWS, CH), bf16), V((14, 2, ROWS, CH), bf16),
        V((NY, ROWS, CH), f32), V((NY, ROWS, CH), bf16), V((3, ROWS, CH), bf16),
        V((NX, 64, CH), f32), V((NX, 64, CH), bf16), V((3, 64, CH), bf16), V((NX, NZ, 64, CH), bf16),
        V((4, 2, ROWS, 256), bf16), V((6, 2, ROWS, 256), bf16),
        V((NY, ROWS, 256), f32), V((NY, ROWS, 256), bf16), V((3, ROWS, 256), bf16),
        V((NZ, 32, 256), f32), V((NZ, 32, 256), bf16), V((7, 32, 256), bf16), V((NX, NZ, 32, 256), bf16),
        V((ROWS, GATED), f32), V((ROWS, GATED), f32),
        pltpu.SemaphoreType.DMA((N_REMOTE,)), pltpu.SemaphoreType.DMA((N_REMOTE,)),
        pltpu.SemaphoreType.DMA((N_LOCAL,)),
    ]
    anywhere = pl.BlockSpec(memory_space=pl.ANY)
    input_grad, up_grad, gate_grad = pl.pallas_call(
        kernel,
        out_shape=(
            jax.ShapeDtypeStruct((ROWS, MODEL), bf16),
            jax.ShapeDtypeStruct((ROWS, GATED), f32),
            jax.ShapeDtypeStruct((ROWS, GATED), f32),
        ),
        in_specs=[anywhere] * 8,
        out_specs=(anywhere,) * 3,
        scratch_shapes=scratch,
        compiler_params=pltpu.CompilerParams(
            collective_id=0, has_side_effects=True, vmem_limit_bytes=60 * 1024 * 1024
        ),
    )(
        inputs, up_pre, gate_pre, cotangent, norm_gain.reshape(1, GATED), up_weight, gate_weight, mix_weight,
    )
    return input_grad[None], up_grad, gate_grad


def solution(mesh):
    return jax.shard_map(
        on_device,
        mesh=mesh,
        in_specs=(
            P("dp", "sp", None),
            P("dp", "sp", None),
            P("dp", "sp", None),
            P("dp", "sp", None),
            P(),
            P("dp", None),
            P("dp", None),
            P(),
        ),
        out_specs=(P("dp", "sp", None), P("dp", None), P("dp", None)),
        check_vma=False,
    )
```

time: 476 us -> 93.6 us (0.20)
  waiting for transfers between devices: 347 us -> 0 us
  Pallas kernels: 0 us -> 87.2 us
  local copies, waits for them, and re-layouts: 63.8 us -> 5.67 us
  matrix products: 19.8 us -> 0 us
  starting transfers between devices: 17.6 us -> 0 us
  between operations: 14 us -> 0.65 us
  other arithmetic: 11.5 us -> 0 us
    psum x1 -> x0, waiting for transfers between devices: 149 us -> none  [on_device(): weight_rows = lax.psum(own_part, 'sp')]
    reduce_scatter x1 -> x0, waiting for transfers between devices: 89.1 us -> none  [on_device(): lax.psum_scatter(lax.dot_general(flat_inputs, both_grads, (((0,), (0,)),...]
    pallas_call x0 -> x1, Pallas kernels: none -> 87.2 us  [on_device(): pl.pallas_call(kernel, out_shape=(jax.ShapeDtypeStruct((ROWS, MODEL), bf1...]
    all_to_all x2 -> x0, waiting for transfers between devices: 54.8 us -> none  [side_by_side(): lax.all_to_all(both, axis, split_axis=split_dim, concat_axis=concat_dim,...]
    all_gather x1 -> x0, waiting for transfers between devices: 54.3 us -> none  [side_by_side_2(): whole = lax.all_gather(both, axis, axis=dim, tiled=True)]
    unnamed x23 -> x5, local copies, waits for them, and re-layouts: 28.3 us -> 5.67 us
    dot_general x5 -> x0, matrix products: 19.8 us -> none  [the longest x1 8.09 us: on_device(): lax.dot_general(flat_inputs, both_grads, (((0,), (0,)), ((), ())), prefer...]
    all_to_all x2 -> x0, starting transfers between devices: 17.3 us -> none  [side_by_side(): lax.all_to_all(both, axis, split_axis=split_dim, concat_axis=concat_dim,...]
  transfers between devices with their start and end apart: 5 -> 0, of which waited for: 5 -> 0; matrix products, arithmetic and copies ran while one was open for 2% -> 0% of each run, Pallas kernels for 0% -> 0%
where the time goes in v1:
time: 93.6 us; the launch traced here: 93.5 us
  Pallas kernels  87.2 us (93%)
  local copies, waits for them, and re-layouts  5.67 us (6%)
    pallas_call x1, Pallas kernels, on_device(): pl.pallas_call(kernel, out_shape=(jax.ShapeDtypeStruct((ROWS, MODEL), bf1...  87.2 us
    unnamed x5, local copies, waits for them, and re-layouts  5.67 us

profile of v1, /device:TPU:2, one launch (start us, length us, event | category | flops | bytes accessed | tf_op | source)
XLA Modules:
  0.0 93.5 jit_solution(5664774965245193864)
XLA Ops:
  0.6 87.2 %shard_map.103 = (bf16[256,2048]{1,0:T(8,128)(2,1)}, f32[256,1024]{1,0:T(8,128)}, f32[256,1024]{1,0:T(8,128)}) custom-call(bf16[1,256,2048]{2,1,0:T(8,128)(2,1)} %x_hbm.1, bf16[1,256,1024]{2,1,0:T(8,128)(2,1)} %up_hbm.1, bf16[1,256,1024]{2,1,0:T(8,128)(2,1)} %gate_hbm.1, bf16[1,256,1024]{2,1,0:T(8,128)(2,1)} %cot_hbm.1, f32[1,1024]{1,0:T(1,128)} %bitcast.3, ...), custom_call_target="tpu_custom_call" | custom-call | tf_op jit(solution)/shard_map/pallas_call | solution.py:514
  87.8 0.0 copy-start
  87.8 2.4 %copy.14 = bf16[1,256,2048]{2,1,0:T(8,128)(2,1)} copy(bf16[1,256,2048]{2,1,0:T(8,128)(2,1)} %bitcast.2) | data formatting | bytes 2097152
  90.2 2.3 %copy.15 = f32[256,1024]{1,0:T(8,128)} copy(f32[256,1024]{1,0:T(8,128)} %get-tuple-element.13) | data formatting | bytes 2097152
  92.5 0.0 copy-done
  92.5 1.0 %copy.16 = f32[256,1024]{1,0:T(8,128)} copy(f32[256,1024]{1,0:T(8,128)S(1)} %copy-done) | data formatting | bytes 2097152
Async XLA Ops:
  87.8 4.7 %copy-start = (f32[256,1024]{1,0:T(8,128)S(1)}, f32[256,1024]{1,0:T(8,128)}, u32[]{:S(2)}) copy-start(f32[256,1024]{1,0:T(8,128)} %get-tuple-element.14) | copy-start | bytes 3145732

commit v2 on v0

v2 whole, which is shorter than its diff:
```python
import math

import jax
import jax.numpy as jnp
from jax import lax
from jax.experimental import pallas as pl
from jax.experimental.pallas import tpu as pltpu
from jax.sharding import PartitionSpec as P

MESH = pl.DeviceIdType.MESH
NX, NY, NZ = 4, 4, 8
ROWS = 256
GATED = 1024
MODEL = 2048
NG = 8
CH = 128
SEG = 64
RB = 16
f32, bf16 = jnp.float32, jnp.bfloat16

norm_eps = 1e-05
grad_scale = 1.0 / 256.0
root_half = 1.0 / math.sqrt(2.0)
root_twopi = 1.0 / math.sqrt(2.0 * math.pi)


def dot(a, b):
    return jnp.dot(a, b, preferred_element_type=f32)


def dot_t(a, b):
    return lax.dot_general(a, b, (((1,), (1,)), ((), ())), preferred_element_type=f32)


class Names:
    def __init__(self):
        self.at = {}

    def __call__(self, *key):
        return self.at.setdefault(key, len(self.at))


N_SEND = 18
N_RECV = 71
N_LOCAL = 7


def kernel(
    x_hbm, up_hbm, gate_hbm, cot_hbm, gainv, wu_hbm, wg_hbm, mix_hbm,
    ig_out, du_out, dg_out,
    upv, gatev, cotv, xo, xp, xt, mixd, mixo, mixin, peer, acc, back, cs, nrm, si,
    gu, gg, wb, uorg, urec, gorg, grec, redf, redb, yrec, subf, subb, ux, gz, agu, agg,
    send_sem, recv_sem, loc_sem,
):
    sp, dp = lax.axis_index("sp"), lax.axis_index("dp")
    z, x = sp // NX, sp % NX
    y, c = dp // 2, dp % 2
    h = x % 2

    def dev(dz=0, dx=0, dy=0, other=False):
        zz, xx, yy = (z + dz + NZ) % NZ, (x + dx + NX) % NX, (y + dy + NY) % NY
        cc = 1 - c if other else c
        return {"sp": zz * NX + xx, "dp": yy * 2 + cc}

    def zi(v):
        return (z + v + NZ) % NZ

    def xi(v):
        return (x + v + NX) % NX

    def yi(v):
        return (y + v + NY) % NY

    pair_dev = {"sp": z * NX + (x + 1 - 2 * h), "dp": dp}
    families, names, held = Names(), Names(), {}

    def bytes_of(ref):
        return math.prod(ref.shape) * ref.dtype.itemsize

    def remote(family, key, src, dst, to):
        return pltpu.make_async_remote_copy(
            src_ref=src, dst_ref=dst, send_sem=send_sem.at[families(family)], recv_sem=recv_sem.at[names(*key)],
            device_id=to, device_id_type=MESH,
        )

    def send(family, key, src, dst, to, note=True):
        remote(family, key, src, dst, to).start()
        if note:
            held[family] = held.get(family, 0) + bytes_of(src)

    def arrive(key, dst):
        pltpu.make_async_copy(dst, dst, recv_sem.at[names(*key)]).wait()

    def all_sent(family, ref):
        assert held.pop(family) == bytes_of(ref), family
        pltpu.make_async_copy(ref, ref, send_sem.at[families(family)]).wait()

    peers = [dev(other=True)]
    peers += [dev(dy=k) for k in range(1, NY)]
    peers += [dev(dx=k) for k in range(1, NX)]
    peers += [dev(dz=k) for k in range(1, NZ)]
    barrier = pltpu.get_barrier_semaphore()
    for p in peers:
        pl.semaphore_signal(barrier, inc=1, device_id=p, device_id_type=MESH)

    local = Names()

    def load(name, src, dst):
        pltpu.make_async_copy(src, dst, loc_sem.at[local(name)]).start()

    def loaded(name, ref):
        pltpu.make_async_copy(ref, ref, loc_sem.at[local(name)]).wait()

    load("gate", gate_hbm.at[0], gatev)
    load("up", up_hbm.at[0], upv)
    load("cot", cot_hbm.at[0], cotv)
    off = pl.multiple_of(h * ROWS, ROWS)
    load("mixd", mix_hbm.at[:, pl.ds(off, ROWS), pl.ds(off, ROWS)], mixd)
    load("mixo", mix_hbm.at[:, pl.ds(ROWS, ROWS), pl.ds(0, ROWS)], mixo)

    def columns(block):
        return pl.ds(pl.multiple_of(block * ROWS, ROWS), ROWS)

    for k in range(NY):
        load("x", x_hbm.at[0, :, columns(2 * k + c)], xo.at[k])
    load("w", wu_hbm, wb.at[dp, 0])
    load("w", wg_hbm, wb.at[dp, 1])

    def gate_rows(i, _):
        rows = pl.ds(pl.multiple_of(i * RB, RB), RB)
        a = gatev[rows, :].astype(f32)
        cdf = 0.5 * (1.0 + lax.erf(a * root_half))
        act = a * cdf
        centered = act - jnp.mean(act, axis=-1, keepdims=True)
        inv = lax.rsqrt(jnp.mean(centered * centered, axis=-1, keepdims=True) + norm_eps)
        normed = centered * inv
        nrm[rows, :] = normed
        si[rows, :] = inv * (cdf + a * jnp.exp(-0.5 * a * a) * root_twopi)
        value = (normed * gainv[...]).astype(bf16)
        for g in range(NG):
            mixin[0, g, rows, :] = value[:, g * CH : (g + 1) * CH]
        return 0

    def up_rows(i, _):
        rows = pl.ds(pl.multiple_of(i * RB, RB), RB)
        a = upv[rows, :].astype(f32)
        ct = cotv[rows, :].astype(f32)
        cdf = 0.5 * (1.0 + lax.erf(a * root_half))
        value = (ct * (a * cdf)).astype(bf16)
        slope = ct * (cdf + a * jnp.exp(-0.5 * a * a) * root_twopi)
        for g in range(NG):
            mixin[1, g, rows, :] = value[:, g * CH : (g + 1) * CH]
            cs[g, rows, :] = slope[:, g * CH : (g + 1) * CH]
        return 0

    loaded("gate", gatev)
    lax.fori_loop(0, ROWS // RB, gate_rows, 0, unroll=4)
    loaded("up", upv)
    loaded("cot", cotv)
    lax.fori_loop(0, ROWS // RB, up_rows, 0)
    pl.semaphore_wait(barrier, len(peers))

    order = [zi(v) for v in (4, 3, -3, 2, -2, 1, -1, 0)]
    for j, g in enumerate(order):
        send("pair", ("pair", j), mixin.at[h, g], peer.at[j], pair_dev)

    mine = {0: wu_hbm, 1: wg_hbm}
    for d, parts in ((1, (0, 1)), (-1, (1, 0))):
        for part in parts:
            send("w", ("w", d, part), mine[part], wb.at[dp, part], dev(dy=d))
    for k in range(NY):
        send("xp", ("xp",), x_hbm.at[0, :, columns(2 * k + 1 - c)], xp.at[k], dev(other=True))

    def block_of(dy, other=False):
        return yi(dy) * 2 + (1 - c if other else c)

    def weights_own():
        for part in range(2):
            send("wc", ("wc", 0), mine[part], wb.at[dp, part], dev(other=True))

    def weights_first():
        for d, part in ((1, 0), (-1, 1)):
            b = block_of(-d)
            arrive(("w", d, part), wb.at[b, part])
            send("wc", ("wc", -d), wb.at[b, part], wb.at[b, part], dev(other=True))

    def weights_pass(f):
        rows = pl.ds(f * 64, 64)
        for d, part in ((1, 0), (-1, 1)):
            b = block_of(-d)
            send("wf", ("wf", f), wb.at[b, part, rows], wb.at[b, part, rows], dev(dy=d))

    def weights_second():
        for d, part in ((1, 1), (-1, 0)):
            b = block_of(-d)
            arrive(("w", d, part), wb.at[b, part])
            send("wc", ("wc", -d), wb.at[b, part], wb.at[b, part], dev(other=True))

    def weights_third(f):
        b, rows = block_of(2), pl.ds(f * 64, 64)
        arrive(("wf", f), wb.at[b, :, rows])
        send("wc", ("wc", 2), wb.at[b, :, rows], wb.at[b, :, rows], dev(other=True))

    def weights_other(dy):
        b = block_of(dy, True)
        arrive(("wc", dy), wb.at[b])

    own, theirs = pl.ds(0, ROWS), pl.ds(ROWS, ROWS)
    loaded("mixd", mixd)
    loaded("mixo", mixo)
    seg_t = lax.broadcasted_iota(jnp.int32, (ROWS, ROWS), 0) // SEG
    seg_s = lax.broadcasted_iota(jnp.int32, (ROWS, ROWS), 1) // SEG
    keep = seg_s <= seg_t

    def diag(g):
        return jnp.where(keep, mixd[g].astype(f32), 0.0)

    def up_grad(g, spatial):
        gu[g, 0:ROWS, :] = (spatial.astype(bf16).astype(f32) * cs[g]).astype(bf16)

    def share_up(j):
        g = order[j]
        send("gu", ("gu", j), gu.at[g, own], gu.at[g, theirs], dev(other=True), note=False)

    def up_here(j):
        g = order[j]
        arrive(("gu", j), gu.at[g, theirs])

    def gate_grads():
        def rows_of(i, _):
            rows = pl.ds(pl.multiple_of(i * RB, RB), RB)
            nb = jnp.concatenate([back[g, rows, :] for g in range(NG)], axis=1)
            scaled = nb.astype(f32) * gainv[...]
            normed = nrm[rows, :]
            m1 = jnp.mean(scaled, axis=-1, keepdims=True)
            m2 = jnp.mean(scaled * normed, axis=-1, keepdims=True)
            grad = ((scaled - m1 - normed * m2) * si[rows, :]).astype(bf16)
            for g in range(NG):
                gg[g, rows, :] = grad[:, g * CH : (g + 1) * CH]
            return 0

        lax.fori_loop(0, ROWS // RB, rows_of, 0, unroll=4)
        send("gg", ("gg",), gg.at[:, own, :], gg.at[:, theirs, :], dev(other=True), note=False)

    @pl.when(h == 0)
    def _():
        def step(g, _):
            d = diag(g)
            up_grad(g, dot(d.astype(bf16), mixin[0, g]))
            acc[g] = dot(d.T.astype(bf16), mixin[1, g])
            return 0

        lax.fori_loop(0, NG, step, 0)
        for j in range(NG):
            share_up(j)

    @pl.when(h == 1)
    def _():
        def step(g, _):
            d = diag(g)
            back[g] = dot(d.T.astype(bf16), mixin[1, g]).astype(bf16)
            acc[g] = dot(d.astype(bf16), mixin[0, g])
            return 0

        lax.fori_loop(0, NG, step, 0)

    loaded("x", xo)
    arrive(("xp",), xp)
    for k in range(NY):
        xt[k, :, 0:ROWS] = xo[k].T
        xt[k, :, ROWS : 2 * ROWS] = xp[k].T

    def pair_step(j):
        g = order[j]
        arrive(("pair", j), peer.at[j])

        @pl.when(h == 0)
        def _():
            back[g] = (acc[g] + dot(mixo[g].astype(f32).T.astype(bf16), peer[j])).astype(bf16)

        @pl.when(h == 1)
        def _():
            up_grad(g, acc[g] + dot(mixo[g], peer[j]))
            share_up(j)

    def late_gate():
        @pl.when(h == 0)
        def _():
            gate_grads()

    def early_gate():
        @pl.when(h == 1)
        def _():
            gate_grads()

    def gate_here():
        arrive(("gg",), gg.at[:, theirs, :])

    def u_term(k, j):
        return dot(xt[k], gu[j])

    def g_term(s):
        return lambda k, j: dot(xt[k], gg[2 * j + s])

    def half_of(d, kind):
        long = 0 if d == 1 else 1
        return long if kind == "L" else 1 - long

    di = {1: 0, -1: 1}

    def fill(dst, slot, term, half, j, add=False):
        for r in range(2):
            t = term(2 * half + r, j)
            if add:
                t = t + dst[slot, r].astype(f32)
            dst[slot, r] = t.astype(bf16)

    def u_slot(d, kind, k):
        return di[d] * 7 + (k if kind == "L" else 4 + k)

    def chain_key(name, d, kind, k):
        return (name, d, kind, k) if k else (name, 0)

    def u_start(kind, dist, directions=(1, -1)):
        for d in directions:
            slot = di[d] * 2 + (0 if kind == "L" else 1)
            fill(uorg, slot, u_term, half_of(d, kind), zi(d * dist))
            send("u", chain_key("u", d, kind, dist - 1), uorg.at[slot], urec.at[u_slot(d, kind, dist - 1)], dev(dz=d))

    def u_step(kind, k):
        for d in (1, -1):
            slot = u_slot(d, kind, k)
            arrive(("u", d, kind, k), urec.at[slot])
            fill(urec, slot, u_term, half_of(d, kind), zi(d * k), add=True)
            send("u", chain_key("u", d, kind, k - 1), urec.at[slot], urec.at[u_slot(d, kind, k - 1)], dev(dz=d))

    def g_slot(s, d, kind, k):
        return s * 6 + di[d] * 3 + (k if kind == "L" else 2)

    def g_start(s, kind, dist):
        for d in (1, -1):
            slot = s * 4 + di[d] * 2 + (0 if kind == "L" else 1)
            fill(gorg, slot, g_term(s), half_of(d, kind), xi(d * dist))
            send("g", chain_key(("g", s), d, kind, dist - 1), gorg.at[slot], grec.at[g_slot(s, d, kind, dist - 1)], dev(dx=d))

    def g_step(s):
        for d in (1, -1):
            slot = g_slot(s, d, "L", 1)
            arrive(chain_key(("g", s), d, "L", 1), grec.at[slot])
            fill(grec, slot, g_term(s), half_of(d, "L"), xi(d), add=True)
            send("g", chain_key(("g", s), d, "L", 0), grec.at[slot], grec.at[g_slot(s, d, "L", 0)], dev(dx=d))

    def y_slot(d, kind, k):
        return di[d] * 3 + (k if kind == "L" else 2)

    def y_rows(d, kind):
        return pl.ds(half_of(d, kind) * 128, 128)

    def close(s, rec, slot_of, key, term, j):
        arrive(key, rec.at[pl.ds(0, 4)])
        for half in range(2):
            plus = slot_of(1, "L" if half == 0 else "S")
            minus = slot_of(-1, "L" if half == 1 else "S")
            for r in range(2):
                k = 2 * half + r
                t = term(k, j) + rec[plus, r].astype(f32) + rec[minus, r].astype(f32)
                redf[s, k] = t
                redb[s, k] = t.astype(bf16)
        for kind, dist in (("L", 2), ("S", 1)):
            for d in (1, -1):
                rows = y_rows(d, kind)
                send("y", chain_key(("y", s), d, kind, dist - 1), redb.at[s, yi(d * dist), rows], yrec.at[s, y_slot(d, kind, dist - 1)], dev(dy=d))

    def u_end():
        close(2, urec, lambda d, kind: u_slot(d, kind, 0), ("u", 0), u_term, z)

    def g_end(s):
        close(s, grec, lambda d, kind: g_slot(s, d, kind, 0), (("g", s), 0), g_term(s), x)

    def y_step(s):
        for d in (1, -1):
            slot, rows = y_slot(d, "L", 1), y_rows(d, "L")
            arrive(chain_key(("y", s), d, "L", 1), yrec.at[s, slot])
            yrec[s, slot] = (yrec[s, slot].astype(f32) + redf[s, yi(d), rows, :]).astype(bf16)
            send("y", chain_key(("y", s), d, "L", 0), yrec.at[s, slot], yrec.at[s, y_slot(d, "L", 0)], dev(dy=d))

    def y_sum(s):
        arrive((("y", s), 0), yrec.at[s, pl.ds(0, 4)])
        for half in range(2):
            plus = y_slot(1, "L" if half == 0 else "S", 0)
            minus = y_slot(-1, "L" if half == 1 else "S", 0)
            rows = pl.ds(half * 128, 128)
            t = redf[s, y, rows, :] + yrec[s, plus].astype(f32) + yrec[s, minus].astype(f32)
            subf[s, rows, :] = t
            subb[s, rows, :] = t.astype(bf16)

    def rows64(v):
        return pl.ds(pl.multiple_of(v * 64, 64), 64)

    def rows32(v):
        return pl.ds(pl.multiple_of(v * 32, 32), 32)

    def y_end(s):
        y_sum(s)
        if s == 2:
            for k in range(1, NX):
                send("ux", ("ux",), subb.at[2, rows64(xi(k))], ux.at[k - 1], dev(dx=k))
        else:
            for k in range(1, NZ):
                send("gz", ("gz", s), subb.at[s, rows32(zi(k))], gz.at[s, k - 1], dev(dz=k))

    def piece_u():
        arrive(("ux",), ux)
        t = subf[2, rows64(x), :]
        for k in range(1, NX):
            t = t + ux[k - 1].astype(f32)
        agu[x, z] = t.astype(bf16)
        for k in range(1, NZ):
            send("au", ("a", 2), agu.at[x, z], agu.at[x, z], dev(dz=k))

    def piece_g(s):
        arrive(("gz", s), gz.at[s])
        t = subf[s, rows32(z), :]
        for k in range(1, NZ):
            t = t + gz[s, k - 1].astype(f32)
        agg[s, x, z] = t.astype(bf16)
        for k in range(1, NZ):
            send("ag", ("a", s), agg.at[s, x, z], agg.at[s, x, z], dev(dz=k))

    def gathered(s):
        return agu if s == 2 else agg.at[s]

    def gather_z(s):
        buf = gathered(s)
        arrive(("a", s), buf.at[0, pl.ds(0, NZ - 1)])
        for d in (1, -1):
            send("axu" if s == 2 else "axg", ("ax", s, d), buf.at[x], buf.at[x], dev(dx=d))

    def part_of(d):
        return pl.ds(0, NZ // 2) if d == 1 else pl.ds(NZ // 2, NZ // 2)

    def gather_x(s):
        buf = gathered(s)
        for d in (1, -1):
            arrive(("ax", s, d), buf.at[xi(-d)])
            send("axxu" if s == 2 else "axxg", ("axx", s), buf.at[xi(-d), part_of(d)], buf.at[xi(-d), part_of(d)], dev(dx=d))

    def gather_last(s):
        arrive(("axx", s), gathered(s).at[xi(2)])

    def out_block(b):
        lu = jnp.concatenate([gu[g, 0:ROWS, :] for g in range(NG)], axis=1)
        lg = jnp.concatenate([gg[g, 0:ROWS, :] for g in range(NG)], axis=1)
        ig_out[:, columns(b)] = (dot_t(lu, wb[b, 0]) + dot_t(lg, wb[b, 1])).astype(bf16)

    def put_up():
        for i in range(NX):
            for j in range(NZ):
                du_out[i * 64 : (i + 1) * 64, j * CH : (j + 1) * CH] = agu[i, j]

    def put_gate():
        for s in range(2):
            for i in range(NX):
                for j in range(NZ):
                    at = (2 * i + s) * CH
                    dg_out[j * 32 : (j + 1) * 32, at : at + CH] = agg[s, i, j]

    def finish_waits():
        held["gu"], held["gg"] = bytes_of(gu.at[:, own]), bytes_of(gg.at[:, own])
        for family, ref in (
            ("pair", mixin.at[0]), ("w", wb.at[pl.ds(0, 2)]), ("xp", xp), ("wc", wb.at[pl.ds(0, 4)]), ("wf", wb.at[0]),
            ("gu", gu.at[:, own]), ("gg", gg.at[:, own]), ("u", urec), ("g", grec), ("y", yrec), ("ux", ux), ("gz", gz),
            ("au", agu.at[0, pl.ds(0, NZ - 1)]), ("ag", agg.at[:, 0, pl.ds(0, NZ - 1)]),
            ("axu", agu.at[pl.ds(0, 2)]), ("axg", agg.at[:, pl.ds(0, 2)]), ("axxu", agu.at[0]), ("axxg", agg.at[:, 0]),
        ):
            all_sent(family, ref)
        assert not held

    pair_step(0)
    up_here(0)
    u_start("L", 4)
    pair_step(1)
    up_here(1)
    u_start("S", 3, (1,))
    pair_step(2)
    up_here(2)
    u_start("S", 3, (-1,))
    early_gate()
    weights_own()
    pair_step(3)
    pair_step(4)
    up_here(3)
    up_here(4)
    u_step("L", 3)
    pair_step(5)
    pair_step(6)
    pair_step(7)
    late_gate()
    gate_here()
    g_start(0, "L", 2)
    u_step("S", 2)
    g_start(0, "S", 1)
    g_start(1, "L", 2)
    up_here(5)
    up_here(6)
    up_here(7)
    u_step("L", 2)
    weights_first()
    weights_pass(0)
    g_step(0)
    g_start(1, "S", 1)
    u_step("S", 1)
    loaded("w", wb.at[dp])
    out_block(block_of(0))
    u_step("L", 1)
    weights_other(0)
    out_block(block_of(0, True))
    g_step(1)
    weights_second()
    g_end(0)
    u_end()
    out_block(block_of(1))
    y_step(0)
    y_step(2)
    g_end(1)
    y_end(0)
    y_end(2)
    weights_pass(1)
    out_block(block_of(3))
    y_step(1)
    weights_other(1)
    out_block(block_of(1, True))
    piece_g(0)
    y_end(1)
    weights_pass(2)
    weights_pass(3)
    piece_u()
    weights_other(-1)
    out_block(block_of(3, True))
    gather_z(0)
    piece_g(1)
    gather_z(2)
    weights_third(0)
    gather_x(0)
    weights_third(1)
    gather_z(1)
    gather_x(2)
    weights_third(2)
    gather_last(0)
    weights_third(3)
    gather_x(1)
    out_block(block_of(2))
    gather_last(2)
    put_up()
    weights_other(2)
    out_block(block_of(2, True))
    gather_last(1)
    put_gate()
    finish_waits()
    assert (len(families.at), len(names.at), len(local.at)) == (N_SEND, N_RECV, N_LOCAL), (len(families.at), len(names.at), len(local.at))


def on_device(inputs, up_pre, gate_pre, cotangent, norm_gain, up_weight, gate_weight, mix_weight):
    V = pltpu.VMEM
    scratch = [
        V((ROWS, GATED), bf16), V((ROWS, GATED), bf16), V((ROWS, GATED), bf16),
        V((NY, ROWS, ROWS), bf16), V((NY, ROWS, ROWS), bf16), V((NY, ROWS, 2 * ROWS), bf16),
        V((NG, ROWS, ROWS), bf16), V((NG, ROWS, ROWS), bf16),
        V((2, NG, ROWS, CH), bf16), V((NG, ROWS, CH), bf16), V((NG, ROWS, CH), f32), V((NG, ROWS, CH), bf16),
        V((NG, ROWS, CH), f32), V((ROWS, GATED), f32), V((ROWS, GATED), f32),
        V((NG, 2 * ROWS, CH), bf16), V((NG, 2 * ROWS, CH), bf16),
        V((8, 2, ROWS, GATED), bf16),
        V((4, 2, ROWS, CH), bf16), V((14, 2, ROWS, CH), bf16),
        V((8, 2, ROWS, CH), bf16), V((12, 2, ROWS, CH), bf16),
        V((3, NY, ROWS, CH), f32), V((3, NY, ROWS, CH), bf16), V((3, 6, 128, CH), bf16),
        V((3, ROWS, CH), f32), V((3, ROWS, CH), bf16),
        V((3, 64, CH), bf16), V((2, 7, 32, CH), bf16), V((NX, NZ, 64, CH), bf16), V((2, NX, NZ, 32, CH), bf16),
        pltpu.SemaphoreType.DMA((N_SEND,)), pltpu.SemaphoreType.DMA((N_RECV,)),
        pltpu.SemaphoreType.DMA((N_LOCAL,)),
    ]
    anywhere = pl.BlockSpec(memory_space=pl.ANY)
    inside = pl.BlockSpec(memory_space=pltpu.VMEM)
    input_grad, up_grad, gate_grad = pl.pallas_call(
        kernel,
        out_shape=(
            pltpu.VMEM((ROWS, MODEL), bf16),
            pltpu.VMEM((ROWS, GATED), bf16),
            pltpu.VMEM((ROWS, GATED), bf16),
        ),
        in_specs=[anywhere] * 4 + [inside] + [anywhere] * 3,
        out_specs=(inside,) * 3,
        scratch_shapes=scratch,
        compiler_params=pltpu.CompilerParams(
            collective_id=0, has_side_effects=True, vmem_limit_bytes=67043328 - 2097152 - 65536
        ),
    )(
        inputs, up_pre, gate_pre, cotangent, norm_gain.reshape(1, GATED), up_weight, gate_weight, mix_weight,
    )
    hbm = pl.BlockSpec(memory_space=pl.ANY)
    return pl.pallas_call(
        widen,
        out_shape=(
            jax.ShapeDtypeStruct((1, ROWS, MODEL), bf16),
            jax.ShapeDtypeStruct((ROWS, GATED), f32),
            jax.ShapeDtypeStruct((ROWS, GATED), f32),
        ),
        in_specs=[inside] * 3,
        out_specs=(hbm,) * 3,
        scratch_shapes=[V((ROWS, GATED), f32), V((ROWS, GATED), f32), pltpu.SemaphoreType.DMA((5,))],
        compiler_params=pltpu.CompilerParams(vmem_limit_bytes=8 * 1024 * 1024),
    )(input_grad, up_grad, gate_grad)


def widen(ig, du, dg, ig_out, du_out, dg_out, duw, dgw, sem):
    copies = [pltpu.make_async_copy(ig, ig_out.at[0], sem.at[0])]
    copies[0].start()
    half = ROWS // 2
    for k, (src, mid, dst) in enumerate(((du, duw, du_out), (dg, dgw, dg_out))):
        for r in range(2):
            rows = pl.ds(r * half, half)
            mid[rows, :] = src[rows, :].astype(f32) * grad_scale
            copies.append(pltpu.make_async_copy(mid.at[rows], dst.at[rows], sem.at[1 + 2 * k + r]))
            copies[-1].start()
    for copy in copies:
        copy.wait()


def solution(mesh):
    return jax.shard_map(
        on_device,
        mesh=mesh,
        in_specs=(
            P("dp", "sp", None),
            P("dp", "sp", None),
            P("dp", "sp", None),
            P("dp", "sp", None),
            P(),
            P("dp", None),
            P("dp", None),
            P(),
        ),
        out_specs=(P("dp", "sp", None), P("dp", None), P("dp", None)),
        check_vma=False,
    )
```

time: 476 us -> 74.8 us (0.16)
  waiting for transfers between devices: 347 us -> 0 us
  Pallas kernels: 0 us -> 73.8 us
  local copies, waits for them, and re-layouts: 63.8 us -> 0 us
  matrix products: 19.8 us -> 0 us
  starting transfers between devices: 17.6 us -> 0 us
  between operations: 14 us -> 0.8 us
  other arithmetic: 11.5 us -> 0 us
    psum x1 -> x0, waiting for transfers between devices: 149 us -> none  [on_device(): weight_rows = lax.psum(own_part, 'sp')]
    reduce_scatter x1 -> x0, waiting for transfers between devices: 89.1 us -> none  [on_device(): lax.psum_scatter(lax.dot_general(flat_inputs, both_grads, (((0,), (0,)),...]
    pallas_call x0 -> x2, Pallas kernels: none -> 73.8 us  [the longest x1 72.1 us: on_device(): pl.pallas_call(kernel, out_shape=(pltpu.VMEM((ROWS, MODEL), bf16), pltpu....]
    all_to_all x2 -> x0, waiting for transfers between devices: 54.8 us -> none  [side_by_side(): lax.all_to_all(both, axis, split_axis=split_dim, concat_axis=concat_dim,...]
    all_gather x1 -> x0, waiting for transfers between devices: 54.3 us -> none  [side_by_side_2(): whole = lax.all_gather(both, axis, axis=dim, tiled=True)]
    unnamed x23 -> x0, local copies, waits for them, and re-layouts: 28.3 us -> none
    dot_general x5 -> x0, matrix products: 19.8 us -> none  [the longest x1 8.09 us: on_device(): lax.dot_general(flat_inputs, both_grads, (((0,), (0,)), ((), ())), prefer...]
    all_to_all x2 -> x0, starting transfers between devices: 17.3 us -> none  [side_by_side(): lax.all_to_all(both, axis, split_axis=split_dim, concat_axis=concat_dim,...]
  transfers between devices with their start and end apart: 5 -> 0, of which waited for: 5 -> 0; matrix products, arithmetic and copies ran while one was open for 2% -> 0% of each run, Pallas kernels for 0% -> 0%
where the time goes in v2:
time: 74.8 us; the launch traced here: 74.6 us
  Pallas kernels  73.8 us (99%)
  between operations  0.8 us (1%)
    pallas_call x1, Pallas kernels, on_device(): pl.pallas_call(kernel, out_shape=(pltpu.VMEM((ROWS, MODEL), bf16), pltpu....  72.1 us
    pallas_call x1, Pallas kernels, on_device(): pl.pallas_call(widen, out_shape=(jax.ShapeDtypeStruct((1, ROWS, MODEL), b...  1.7 us

profile of v2, /device:TPU:2, one launch (start us, length us, event | category | flops | bytes accessed | tf_op | source)
XLA Modules:
  0.0 74.6 jit_solution(13871462670272603626)
XLA Ops:
  0.6 72.1 %shard_map.103 = (bf16[256,2048]{1,0:T(8,128)(2,1)S(1)}, bf16[256,1024]{1,0:T(8,128)(2,1)S(1)}, bf16[256,1024]{1,0:T(8,128)(2,1)S(1)}) custom-call(bf16[1,256,2048]{2,1,0:T(8,128)(2,1)} %x_hbm.1, bf16[1,256,1024]{2,1,0:T(8,128)(2,1)} %up_hbm.1, bf16[1,256,1024]{2,1,0:T(8,128)(2,1)} %gate_hbm.1, bf16[1,256,1024]{2,1,0:T(8,128)(2,1)} %cot_hbm.1, ...), custom_call_target="tpu_custom_call" | custom-call | tf_op jit(solution)/shard_map/pallas_call | solution.py:583
  72.8 1.7 %shard_map.104 = (bf16[1,256,2048]{2,1,0:T(8,128)(2,1)}, f32[256,1024]{1,0:T(8,128)}, f32[256,1024]{1,0:T(8,128)}) custom-call(bf16[256,2048]{1,0:T(8,128)(2,1)S(1)} %get-tuple-element.6.ig, bf16[256,1024]{1,0:T(8,128)(2,1)S(1)} %get-tuple-element.7.du, bf16[256,1024]{1,0:T(8,128)(2,1)S(1)} %get-tuple-element.8.dg), custom_call_target="tpu_custom_call" | custom-call | tf_op jit(solution)/shard_map/pallas_call | solution.py:600

commit v3 on v2

--- a/solution.py
+++ b/solution.py
@@ -153,11 +153,17 @@
             cs[g, rows, :] = slope[:, g * CH : (g + 1) * CH]
         return 0
 
-    loaded("gate", gatev)
-    lax.fori_loop(0, ROWS // RB, gate_rows, 0, unroll=4)
-    loaded("up", upv)
-    loaded("cot", cotv)
-    lax.fori_loop(0, ROWS // RB, up_rows, 0)
+    def gate_side():
+        loaded("gate", gatev)
+        lax.fori_loop(0, ROWS // RB, gate_rows, 0, unroll=4)
+
+    def up_side():
+        loaded("up", upv)
+        loaded("cot", cotv)
+        lax.fori_loop(0, ROWS // RB, up_rows, 0)
+
+    pl.when(h == 0)(gate_side)
+    pl.when(h == 1)(up_side)
     pl.semaphore_wait(barrier, len(peers))
 
     order = [zi(v) for v in (4, 3, -3, 2, -2, 1, -1, 0)]
@@ -170,6 +176,9 @@
             send("w", ("w", d, part), mine[part], wb.at[dp, part], dev(dy=d))
     for k in range(NY):
         send("xp", ("xp",), x_hbm.at[0, :, columns(2 * k + 1 - c)], xp.at[k], dev(other=True))
+
+    pl.when(h == 0)(up_side)
+    pl.when(h == 1)(gate_side)
 
     def block_of(dy, other=False):
         return yi(dy) * 2 + (1 - c if other else c)
@@ -480,78 +489,78 @@
     up_here(0)
     u_start("L", 4)
     pair_step(1)
+    pair_step(2)
     up_here(1)
     u_start("S", 3, (1,))
-    pair_step(2)
     up_here(2)
     u_start("S", 3, (-1,))
-    early_gate()
-    weights_own()
     pair_step(3)
     pair_step(4)
+    u_step("L", 3)
+    pair_step(5)
+    early_gate()
+    pair_step(6)
     up_here(3)
     up_here(4)
-    u_step("L", 3)
-    pair_step(5)
-    pair_step(6)
+    u_step("S", 2)
     pair_step(7)
     late_gate()
     gate_here()
     g_start(0, "L", 2)
-    u_step("S", 2)
     g_start(0, "S", 1)
-    g_start(1, "L", 2)
+    weights_own()
     up_here(5)
     up_here(6)
     up_here(7)
     u_step("L", 2)
+    g_start(1, "L", 2)
     weights_first()
     weights_pass(0)
+    u_step("S", 1)
     g_step(0)
     g_start(1, "S", 1)
-    u_step("S", 1)
+    u_step("L", 1)
     loaded("w", wb.at[dp])
     out_block(block_of(0))
-    u_step("L", 1)
     weights_other(0)
     out_block(block_of(0, True))
     g_step(1)
     weights_second()
+    u_end()
     g_end(0)
-    u_end()
     out_block(block_of(1))
+    y_step(2)
     y_step(0)
-    y_step(2)
     g_end(1)
+    y_end(2)
     y_end(0)
-    y_end(2)
-    weights_pass(1)
     out_block(block_of(3))
     y_step(1)
-    weights_other(1)
-    out_block(block_of(1, True))
+    weights_pass(1)
+    piece_u()
     piece_g(0)
     y_end(1)
     weights_pass(2)
     weights_pass(3)
-    piece_u()
+    weights_other(1)
+    out_block(block_of(1, True))
+    gather_z(2)
+    gather_z(0)
+    piece_g(1)
     weights_other(-1)
     out_block(block_of(3, True))
-    gather_z(0)
-    piece_g(1)
-    gather_z(2)
+    gather_x(2)
+    gather_x(0)
     weights_third(0)
-    gather_x(0)
+    gather_z(1)
     weights_third(1)
-    gather_z(1)
-    gather_x(2)
-    weights_third(2)
-    gather_last(0)
-    weights_third(3)
-    gather_x(1)
-    out_block(block_of(2))
     gather_last(2)
     put_up()
+    weights_third(2)
+    weights_third(3)
+    out_block(block_of(2))
+    gather_x(1)
+    gather_last(0)
     weights_other(2)
     out_block(block_of(2, True))
     gather_last(1)

time: 74.8 us -> 72.5 us (0.969)
  Pallas kernels: 73.8 us -> 71.6 us
    pallas_call x1, Pallas kernels: 72.1 us -> 69.9 us  [on_device(): pl.pallas_call(kernel, out_shape=(pltpu.VMEM((ROWS, MODEL), bf16), pltpu....]
where the time goes in v3:
time: 72.5 us; the launch traced here: 72.4 us
  Pallas kernels  71.6 us (99%)
  between operations  0.8 us (1%)
    pallas_call x1, Pallas kernels, on_device(): pl.pallas_call(kernel, out_shape=(pltpu.VMEM((ROWS, MODEL), bf16), pltpu....  69.9 us
    pallas_call x1, Pallas kernels, on_device(): pl.pallas_call(widen, out_shape=(jax.ShapeDtypeStruct((1, ROWS, MODEL), b...  1.7 us

profile of v3, /device:TPU:2, one launch (start us, length us, event | category | flops | bytes accessed | tf_op | source)
XLA Modules:
  0.0 72.4 jit_solution(752981623358107400)
XLA Ops:
  0.6 69.9 %shard_map.103 = (bf16[256,2048]{1,0:T(8,128)(2,1)S(1)}, bf16[256,1024]{1,0:T(8,128)(2,1)S(1)}, bf16[256,1024]{1,0:T(8,128)(2,1)S(1)}) custom-call(bf16[1,256,2048]{2,1,0:T(8,128)(2,1)} %x_hbm.1, bf16[1,256,1024]{2,1,0:T(8,128)(2,1)} %up_hbm.1, bf16[1,256,1024]{2,1,0:T(8,128)(2,1)} %gate_hbm.1, bf16[1,256,1024]{2,1,0:T(8,128)(2,1)} %cot_hbm.1, ...), custom_call_target="tpu_custom_call" | custom-call | tf_op jit(solution)/shard_map/pallas_call | solution.py:592
  70.5 1.7 %shard_map.104 = (bf16[1,256,2048]{2,1,0:T(8,128)(2,1)}, f32[256,1024]{1,0:T(8,128)}, f32[256,1024]{1,0:T(8,128)}) custom-call(bf16[256,2048]{1,0:T(8,128)(2,1)S(1)} %get-tuple-element.6.ig, bf16[256,1024]{1,0:T(8,128)(2,1)S(1)} %get-tuple-element.7.du, bf16[256,1024]{1,0:T(8,128)(2,1)S(1)} %get-tuple-element.8.dg), custom_call_target="tpu_custom_call" | custom-call | tf_op jit(solution)/shard_map/pallas_call | solution.py:609
